TPU v7x, 32 devices: a whole 2x2x4 slice. The times are simulated.
32 devices in a mesh: sp: 8 (over z, core), tp: 4 (over y, x).
Axes of the slice: x: 2, y: 2, z: 4, core: 2. Of those that a mesh axis runs over, the one named last changes fastest.
Arguments:
- residual_in: bfloat16 [2048, 2048], P('sp'), may hold values from -3 to 3
- mix_gain: float32 [2048], replicated, may hold values from 0.1 to 1.9
- pool_weight: bfloat16 [512, 2048], P(None, 'tp'), may hold values from -0.5 to 0.5
- pool_scale: float32 [2048], P('tp'), may hold values from 0.1 to 1.9
- ffn_gain: float32 [2048], replicated, may hold values from 0.1 to 1.9
- route_ids: int32 [2048, 2], P('sp'), may hold values from 0 to 7, all different within a row; in each aligned block of 64 rows (0 to 63, 64 to 127, ...) at most 32 rows name the same one
- route_weights: float32 [2048, 2], P('sp'), may hold values from 0.1 to 1
- gate_weight: bfloat16 [8, 2048, 3584], P('sp', None, 'tp'), may hold values from -0.125 to 0.125
- up_weight: bfloat16 [8, 2048, 3584], P('sp', None, 'tp'), may hold values from -0.125 to 0.125
- down_weight: bfloat16 [8, 3584, 2048], P('sp', 'tp'), may hold values from -0.09375 to 0.09375
Outputs:
- layer_out: bfloat16 [2048, 2048], P('sp')
Inputs may be any that keep to these rules, and one draw needn't show every extreme that they name: `route_ids`: each row names 2 different experts; in each aligned block of 64 rows no expert is named by more than 32 rows, and some block has an expert named by exactly 32 rows.
All inputs are finite; a program needn't handle non-finite values.
Results may differ from a plain program's by a relative error of at most 0.0074.
Values may be sent and summed in bfloat16 or wider, within the bound.
A program may use at most 64 MiB of HBM per device.

v0:
```python
import jax
import jax.numpy as jnp
from jax import lax
from jax.sharding import PartitionSpec as P

GROUPS = 4
SPAN = 16
TOP_K = 2
EPS = 1e-06


def from_behind(value, axis, steps):
    count = lax.axis_size(axis)
    first, last = (max(0, -steps), min(count, count - steps))
    return lax.ppermute(value, axis, [(source, source + steps) for source in range(first, last)])


def rms_scale(values, gain):
    return values * lax.rsqrt(jnp.mean(values * values, axis=-1, keepdims=True) + EPS) * gain


def slot_table(chosen_ids, experts, capacity):
    flat_ids = chosen_ids.reshape(-1)
    matches = (flat_ids[:, None] == jnp.arange(experts, dtype=jnp.int32)[None, :]).astype(jnp.int32)
    before = jnp.cumsum(matches, axis=0) - matches
    slot_of = jnp.sum(before * matches, axis=1)
    target = flat_ids * capacity + slot_of
    return (target[:, None] == jnp.arange(experts * capacity, dtype=jnp.int32)[None, :]).astype(
        jnp.float32
    )


def shards(
    residual_in,
    mix_gain,
    pool_weight,
    pool_scale,
    ffn_gain,
    route_ids,
    route_weights,
    gate_weight,
    up_weight,
    down_weight,
):
    tp_count = lax.axis_size("tp")
    sp_count = lax.axis_size("sp")
    tp_index = lax.axis_index("tp")
    tok_count, width = residual_in.shape
    group_width = width // GROUPS
    col_count = pool_weight.shape[1]
    row_count = tok_count // tp_count
    capacity = 2 * TOP_K * row_count // sp_count
    group_index = tp_index * col_count // group_width
    window = jnp.power(2, group_index + 1)
    stream = residual_in.astype(jnp.float32)
    inverse = lax.rsqrt(jnp.mean(stream * stream, axis=-1, keepdims=True) + EPS)
    stream_group = lax.dynamic_slice_in_dim(stream, group_index * group_width, group_width, 1)
    gain_group = lax.dynamic_slice_in_dim(mix_gain, group_index * group_width, group_width, 0)
    normed_group = (stream_group * inverse * gain_group).astype(jnp.bfloat16)
    rim_rows = from_behind(normed_group[tok_count - SPAN :], "sp", 1)
    extended = jnp.concatenate([rim_rows, normed_group], axis=0).astype(jnp.float32)
    window_sum = jnp.zeros((tok_count, group_width), jnp.float32)
    for offset in range(SPAN):
        window_sum = window_sum + jnp.where(
            offset < window, extended[SPAN - offset : SPAN - offset + tok_count], 0.0
        )
    position = lax.axis_index("sp") * tok_count + jnp.arange(tok_count, dtype=jnp.int32)
    divisor = jnp.minimum(position + 1, window).astype(jnp.float32)
    pooled = (window_sum / divisor[:, None] - extended[SPAN:]).astype(jnp.bfloat16)
    mixed = (jnp.dot(pooled, pool_weight, preferred_element_type=jnp.float32) * pool_scale).astype(
        jnp.bfloat16
    )
    stream_own = lax.dynamic_slice_in_dim(stream, tp_index * row_count, row_count, 0)
    mixed_own = lax.all_to_all(mixed, "tp", split_axis=0, concat_axis=1, tiled=True)
    after_own = (stream_own + mixed_own.astype(jnp.float32)).astype(jnp.bfloat16)
    normed_own = rms_scale(after_own.astype(jnp.float32), ffn_gain).astype(jnp.bfloat16)
    ids_own = lax.dynamic_slice_in_dim(route_ids, tp_index * row_count, row_count, 0)
    table_own = slot_table(ids_own, sp_count, capacity)
    repeated = jnp.repeat(normed_own, TOP_K, axis=0)
    outgoing = lax.dot_general(
        table_own.astype(jnp.bfloat16),
        repeated,
        (((0,), (0,)), ((), ())),
        preferred_element_type=jnp.float32,
    )
    outgoing = outgoing.astype(jnp.bfloat16).reshape(sp_count, capacity, width)
    arrived = lax.all_to_all(outgoing, "sp", split_axis=0, concat_axis=0, tiled=True)
    piece = lax.all_gather(arrived, "tp", axis=0, tiled=True)
    flat_rows = piece.reshape(-1, width)
    gate_part = jnp.dot(flat_rows, gate_weight[0], preferred_element_type=jnp.float32)
    up_part = jnp.dot(flat_rows, up_weight[0], preferred_element_type=jnp.float32)
    hidden = (jax.nn.silu(gate_part) * up_part).astype(jnp.bfloat16)
    hidden_all = hidden.reshape(piece.shape[0], piece.shape[1], hidden.shape[1])
    hidden_flat = hidden_all.reshape(-1, hidden_all.shape[-1])
    term = jnp.dot(hidden_flat, down_weight[0], preferred_element_type=jnp.float32)
    summed = lax.psum_scatter(
        term.astype(jnp.bfloat16).astype(jnp.float32).astype(jnp.bfloat16),
        "tp",
        scatter_dimension=0,
        tiled=True,
    )
    expert_out = summed.reshape(sp_count, capacity, width)
    returned_rows = lax.all_to_all(expert_out, "sp", split_axis=0, concat_axis=0, tiled=True)
    weights_own = lax.dynamic_slice_in_dim(route_weights, tp_index * row_count, row_count, 0)
    weight_table = jnp.einsum(
        "rk,rkc->rc", weights_own, table_own.reshape(row_count, TOP_K, sp_count * capacity)
    )
    expert_mix = jnp.dot(
        weight_table,
        returned_rows.reshape(-1, width).astype(jnp.float32),
        precision=lax.Precision.HIGHEST,
    )
    out_own = (after_own.astype(jnp.float32) + expert_mix).astype(jnp.bfloat16)
    return lax.all_gather(out_own, "tp", axis=0, tiled=True)


def solution(mesh):
    placed = (
        P("sp", None),
        P(),
        P(None, "tp"),
        P("tp"),
        P(),
        P("sp", None),
        P("sp", None),
        P("sp", None, "tp"),
        P("sp", None, "tp"),
        P("sp", "tp", None),
    )
    return jax.shard_map(
        shards, mesh=mesh, in_specs=placed, out_specs=P("sp", None), check_vma=False
    )
```

profile of v0, /device:TPU:0, one launch (start us, length us, event | category | flops | bytes accessed | tf_op | source)
XLA Modules:
  0.0 247.7 jit_solution(884471469957618278)
XLA Ops:
  6.5 1.6 convert_element_type.65
  8.2 0.3 multiply_reduce_fusion
  8.5 0.8 dynamic_slice.17
  9.2 0.1 multiply_convert_fusion.1
  9.4 2.4 collective-permute-start
  11.9 0.1 copy.19
  12.0 0.1 eq.35
  12.2 0.2 reduce_window_sum.11
  12.4 0.2 select_reduce_fusion
  12.7 2.0 fusion.8
  14.7 4.7 %all-to-all-start = ((bf16[4,64,512]{2,1,0:T(8,128)(2,1)}), bf16[4,64,512]{2,1,0:T(8,128)(2,1)S(1)}, u32[]{:S(2)}, u32[]{:S(2)}) async-start(bf16[4,64,512]{2,1,0:T(8,128)(2,1)} %bitcast), calls=%async_computation | async-start | bytes 524288 | tf_op jit(solution)/shard_map/all_to_all | solution.py:74
  19.4 6.0 %all-to-all-done = bf16[4,64,512]{2,1,0:T(8,128)(2,1)S(1)} async-done(((bf16[4,64,512]{2,1,0:T(8,128)(2,1)}), bf16[4,64,512]{2,1,0:T(8,128)(2,1)S(1)}, u32[]{:S(2)}, u32[]{:S(2)}) %all-to-all-start) | async-done | bytes 262176 | tf_op jit(solution)/shard_map/all_to_all | solution.py:74
  25.5 0.2 fusion.9
  25.7 0.1 fusion.11
  25.8 0.3 broadcast_in_dim.32
  26.1 0.2 reshape.66
  26.3 0.5 convolution_convert_fusion.1
  26.9 33.2 %all_to_all.23 = bf16[8,32,2048]{2,1,0:T(8,128)(2,1)} all-to-all(bf16[8,32,2048]{2,1,0:T(8,128)(2,1)S(1)} %bitcast.33), channel_id=1, replica_groups=mesh['sp'=8,'tp'=4] {'sp'}, dimensions={0} | all-to-all | bytes 2097152 | tf_op jit(solution)/shard_map/all_to_all | solution.py:87
  60.1 50.4 %all-gather.3.cloned.1.call-done = bf16[32,32,2048]{2,1,0:T(8,128)(2,1)} async-done(((bf16[8,32,2048]{2,1,0:T(8,128)(2,1)}), bf16[32,32,2048]{2,1,0:T(8,128)(2,1)}) %all-gather.3.cloned.1.call-update) | async-done | bytes 4194320 | tf_op jit(solution)/shard_map/all_gather | solution.py:88
  110.6 7.5 %fusion.1 = f32[1024,896]{1,0:T(8,128)S(1)} fusion(bf16[1024,2048]{1,0:T(8,128)(2,1)} %bitcast.36, bf16[1,2048,896]{2,1,0:T(8,128)(2,1)} %param.18), kind=kOutput, calls=%fused_computation.2 | convolution fusion | flops 3758096384 | bytes 11534336 | tf_op jit(solution)/shard_map/dot_general | solution.py:91
  118.1 4.7 %multiply_convert_fusion = bf16[1024,896]{1,0:T(8,128)(2,1)S(1)} fusion(f32[1024,896]{1,0:T(8,128)S(1)} %fusion.1, bf16[1024,2048]{1,0:T(8,128)(2,1)S(1)} %bitcast.37, bf16[1,2048,896]{2,1,0:T(8,128)(2,1)S(1)} %copy-done.5), kind=kOutput, calls=%fused_computation.6 | convolution fusion | flops 3763601408 | bytes 13369344 | tf_op jit(solution)/shard_map/dot_general | solution.py:90
  122.9 6.0 %convolution_convert_fusion = bf16[1024,2048]{1,0:T(8,128)(2,1)} fusion(bf16[1024,896]{1,0:T(8,128)(2,1)S(1)} %multiply_convert_fusion, bf16[1,896,2048]{2,1,0:T(8,128)(2,1)S(1)} %copy-done.6), kind=kOutput, calls=%fused_computation | convolution fusion | flops 3760193536 | bytes 9699328 | tf_op jit(solution)/shard_map/dot_general | solution.py:95
  128.9 52.8 %reduce-scatter.2.cloned.1.call-done = bf16[256,2048]{1,0:T(8,128)(2,1)} async-done(((bf16[1024,2048]{1,0:T(8,128)(2,1)}), bf16[256,2048]{1,0:T(8,128)(2,1)}) %reduce-scatter.2.cloned.1.call-update) | async-done | bytes 1048592 | tf_op jit(solution)/shard_map/reduce_scatter | solution.py:96
  181.7 4.6 %all-to-all-start.2 = ((bf16[8,32,2048]{2,1,0:T(8,128)(2,1)}), bf16[8,32,2048]{2,1,0:T(8,128)(2,1)S(1)}, u32[]{:S(2)}, u32[]{:S(2)}) async-start(bf16[8,32,2048]{2,1,0:T(8,128)(2,1)} %bitcast.35), calls=%async_computation.3 | async-start | bytes 2097152 | tf_op jit(solution)/shard_map/all_to_all | solution.py:103
  186.3 0.1 reduce_sum.31
  186.5 0.8 dynamic-slice_bitcast_fusion
  187.2 0.1 copy.17
  187.4 0.3 fusion.30
  187.7 25.2 %all-to-all-done.2 = bf16[8,32,2048]{2,1,0:T(8,128)(2,1)S(1)} async-done(((bf16[8,32,2048]{2,1,0:T(8,128)(2,1)}), bf16[8,32,2048]{2,1,0:T(8,128)(2,1)S(1)}, u32[]{:S(2)}, u32[]{:S(2)}) %all-to-all-start.2) | async-done | bytes 1048608 | tf_op jit(solution)/shard_map/all_to_all | solution.py:103
  212.9 1.4 fusion.7
  214.3 24.6 %all-gather.5.cloned.1.call-done = bf16[256,2048]{1,0:T(8,128)(2,1)} async-done(((bf16[64,2048]{1,0:T(8,128)(2,1)}), bf16[256,2048]{1,0:T(8,128)(2,1)}) %all-gather.5.cloned.1.call-update) | async-done | bytes 1048592 | tf_op jit(solution)/shard_map/all_gather | solution.py:114
  238.9 2.3 copy.26
  (34 shorter events, 0.5 us)
Async XLA Ops:
  6.5 6.2 %copy-start = (bf16[512,512]{1,0:T(8,128)(2,1)S(1)}, bf16[512,512]{1,0:T(8,128)(2,1)}, u32[]{:S(2)}) copy-start(bf16[512,512]{1,0:T(8,128)(2,1)} %param.12) | copy-start | bytes 1572868
  6.5 5.3 %copy-start.3 = (s32[256,2]{0,1:T(2,128)S(1)}, s32[256,2]{0,1:T(2,128)}, u32[]{:S(2)}) copy-start(s32[256,2]{0,1:T(2,128)} %param.15) | copy-start | bytes 6148
  6.5 6.2 %copy-start.7 = (f32[512]{0:T(512)S(1)}, f32[512]{0:T(512)}, u32[]{:S(2)}) copy-start(f32[512]{0:T(512)} %param.13) | copy-start | bytes 6148
  6.5 1.6 copy-start.1
  9.4 3.3 %collective-permute-start = (bf16[16,512]{1,0:T(8,128)(2,1)S(1)}, bf16[16,512]{1,0:T(8,128)(2,1)S(1)}, u32[]{:S(2)}, u32[]{:S(2)}) collective-permute-start(bf16[16,512]{1,0:T(8,128)(2,1)S(1)} %slice.69), channel_id=1, source_target_pairs={{0,4},{4,8},{8,12},{12,16},{16,20},{20,24},{24,28},{1,5},{5,9},{9,... | collective-permute-start | bytes 49160 | tf_op jit(solution)/shard_map/ppermute | solution.py:15
  14.7 10.9 %copy-start.2 = (f32[2048]{0:T(1024)S(1)}, f32[2048]{0:T(1024)}, u32[]{:S(2)}) copy-start(f32[2048]{0:T(1024)} %param.14) | copy-start | bytes 24580
  14.7 10.6 %all-to-all-start = ((bf16[4,64,512]{2,1,0:T(8,128)(2,1)}), bf16[4,64,512]{2,1,0:T(8,128)(2,1)S(1)}, u32[]{:S(2)}, u32[]{:S(2)}) async-start(bf16[4,64,512]{2,1,0:T(8,128)(2,1)} %bitcast), calls=%async_computation | async-start | bytes 524288 | tf_op jit(solution)/shard_map/all_to_all | solution.py:74
  19.4 91.1 %all-gather.3.cloned.1.call-start = ((), (), s32[]{:S(2)}) async-start(), calls=%async_computation.4 | async-start | bytes 5242880 | tf_op jit(solution)/shard_map/all_gather | solution.py:88
  60.1 121.6 %reduce-scatter.2.cloned.1.call-start = ((), (), s32[]{:S(2)}) async-start(), calls=%async_computation.5 | async-start | bytes 5242880 | tf_op jit(solution)/shard_map/reduce_scatter | solution.py:96
  110.6 7.5 %copy-start.4 = (bf16[32,32,2048]{2,1,0:T(8,128)(2,1)S(1)}, bf16[32,32,2048]{2,1,0:T(8,128)(2,1)}, u32[]{:S(2)}) copy-start(bf16[32,32,2048]{2,1,0:T(8,128)(2,1)} %all-gather.3.cloned.1.call-done) | copy-start | bytes 12582916
  110.6 7.5 %copy-start.5 = (bf16[1,2048,896]{2,1,0:T(8,128)(2,1)S(1)}, bf16[1,2048,896]{2,1,0:T(8,128)(2,1)}, u32[]{:S(2)}) copy-start(bf16[1,2048,896]{2,1,0:T(8,128)(2,1)} %param.17) | copy-start | bytes 11010052
  118.1 4.8 %copy-start.6 = (bf16[1,896,2048]{2,1,0:T(8,128)(2,1)S(1)}, bf16[1,896,2048]{2,1,0:T(8,128)(2,1)}, u32[]{:S(2)}) copy-start(bf16[1,896,2048]{2,1,0:T(8,128)(2,1)} %param.19) | copy-start | bytes 11010052
  181.7 31.2 %all-to-all-start.2 = ((bf16[8,32,2048]{2,1,0:T(8,128)(2,1)}), bf16[8,32,2048]{2,1,0:T(8,128)(2,1)S(1)}, u32[]{:S(2)}, u32[]{:S(2)}) async-start(bf16[8,32,2048]{2,1,0:T(8,128)(2,1)} %bitcast.35), calls=%async_computation.3 | async-start | bytes 2097152 | tf_op jit(solution)/shard_map/all_to_all | solution.py:103
  186.3 52.6 %all-gather.5.cloned.1.call-start = ((), (), s32[]{:S(2)}) async-start(), calls=%async_computation.6 | async-start | bytes 1310720 | tf_op jit(solution)/shard_map/all_gather | solution.py:114
Sparse Core Ops, SparseCore 0:
  60.2 50.3 all-gather.2
  129.1 52.5 reduce-scatter.1
  214.4 24.4 all-gather.4
where the time goes:
time: 248 us
  waiting for transfers between devices  159 us (64%)
  blocking collectives  33.2 us (13%)
  matrix products  22.5 us (9%)
  between operations  13.4 us (5%)
  starting transfers between devices  11.7 us (5%)
  local copies, waits for them, and re-layouts  5 us (2%)
  other arithmetic  2.84 us (1%)
    reduce_scatter x1, waiting for transfers between devices, shards(): lax.psum_scatter(term.astype(jnp.bfloat16).astype(jnp.float32).astype(jnp...  52.8 us
    all_gather x1, waiting for transfers between devices, shards(): piece = lax.all_gather(arrived, 'tp', axis=0, tiled=True)  50.4 us
    all_to_all x1, blocking collectives, shards(): lax.all_to_all(outgoing, 'sp', split_axis=0, concat_axis=0, tiled=True)  33.2 us
    all_to_all x1, waiting for transfers between devices, shards(): lax.all_to_all(expert_out, 'sp', split_axis=0, concat_axis=0, tiled=True)  25.2 us
    all_gather x1, waiting for transfers between devices, shards(): return lax.all_gather(out_own, 'tp', axis=0, tiled=True)  24.6 us
    dot_general x1, matrix products, shards(): jnp.dot(flat_rows, up_weight[0], preferred_element_type=jnp.float32)  7.49 us
    dot_general x1, matrix products, shards(): jnp.dot(hidden_flat, down_weight[0], preferred_element_type=jnp.float32)  6.05 us
    all_to_all x1, waiting for transfers between devices, shards(): lax.all_to_all(mixed, 'tp', split_axis=0, concat_axis=1, tiled=True)  5.96 us
  transfers between devices with their start and end apart: 6, of which 5 were waited for; matrix products, arithmetic and copies ran while one was open for 1% of the time, Pallas kernels for 0%

commit v1 on v0

--- a/solution.py
+++ b/solution.py
@@ -7,6 +7,22 @@
 SPAN = 16
 TOP_K = 2
 EPS = 1e-06
+
+
+def _derive_quarters(base_x, net_axis):
+    windows = [base_x]
+    b = 0
+    world_n = lax.psum(1, net_axis)
+    while b < world_n - 1:
+        outcome_arr = lax.ppermute(
+            windows[-1], net_axis, perm=[(dev_i, (dev_i + 1) % world_n) for dev_i in range(world_n)]
+        )
+        windows.append(outcome_arr)
+        b = b + 1
+    vec_out = jnp.concatenate(windows[::-1], 0)
+    response = lax.axis_index(net_axis)
+    b_now = jnp.roll(vec_out, (response + 1) * base_x.shape[0], 0)
+    return b_now
 
 
 def from_behind(value, axis, steps):
@@ -85,7 +101,7 @@
     )
     outgoing = outgoing.astype(jnp.bfloat16).reshape(sp_count, capacity, width)
     arrived = lax.all_to_all(outgoing, "sp", split_axis=0, concat_axis=0, tiled=True)
-    piece = lax.all_gather(arrived, "tp", axis=0, tiled=True)
+    piece = _derive_quarters(arrived, "tp")
     flat_rows = piece.reshape(-1, width)
     gate_part = jnp.dot(flat_rows, gate_weight[0], preferred_element_type=jnp.float32)
     up_part = jnp.dot(flat_rows, up_weight[0], preferred_element_type=jnp.float32)

time: 248 us -> 277 us (1.12)
  waiting for transfers between devices: 159 us -> 181 us
  local copies, waits for them, and re-layouts: 5 us -> 12.4 us
  matrix products: 22.5 us -> 19.4 us
    ppermute x0 -> x3, waiting for transfers between devices: none -> 72.5 us  [_derive_quarters(): lax.ppermute(windows[-1], net_axis, perm=[(dev_i, (dev_i + 1) % world_n)...]
    all_gather x1 -> x0, waiting for transfers between devices: 50.4 us -> none  [shards(): piece = lax.all_gather(arrived, 'tp', axis=0, tiled=True)]
    unnamed x18 -> x23, local copies, waits for them, and re-layouts: 2.46 us -> 9.26 us
    dot_general x1, matrix products: 7.49 us -> 4.69 us  [shards(): jnp.dot(flat_rows, up_weight[0], preferred_element_type=jnp.float32)]
  transfers between devices with their start and end apart: 6 -> 8, of which waited for: 5 -> 7; matrix products, arithmetic and copies ran while one was open for 1% -> 1% of each run, Pallas kernels for 0% -> 0%
where the time goes in v1:
time: 277 us
  waiting for transfers between devices  181 us (65%)
  blocking collectives  33.1 us (12%)
  matrix products  19.4 us (7%)
  between operations  13.8 us (5%)
  starting transfers between devices  13.2 us (5%)
  local copies, waits for them, and re-layouts  12.4 us (4%)
  other arithmetic  4.02 us (1%)
    ppermute x3, waiting for transfers between devices, _derive_quarters(): lax.ppermute(windows[-1], net_axis, perm=[(dev_i, (dev_i + 1) % world_n)...  72.5 us
    reduce_scatter x1, waiting for transfers between devices, shards(): lax.psum_scatter(term.astype(jnp.bfloat16).astype(jnp.float32).astype(jnp...  52.3 us
    all_to_all x1, blocking collectives, shards(): lax.all_to_all(outgoing, 'sp', split_axis=0, concat_axis=0, tiled=True)  33.1 us
    all_to_all x1, waiting for transfers between devices, shards(): lax.all_to_all(expert_out, 'sp', split_axis=0, concat_axis=0, tiled=True)  25.2 us
    all_gather x1, waiting for transfers between devices, shards(): return lax.all_gather(out_own, 'tp', axis=0, tiled=True)  24.6 us
    unnamed x23, local copies, waits for them, and re-layouts  9.26 us
    dot_general x1, matrix products, shards(): jnp.dot(hidden_flat, down_weight[0], preferred_element_type=jnp.float32)  6.05 us
    all_to_all x1, waiting for transfers between devices, shards(): lax.all_to_all(mixed, 'tp', split_axis=0, concat_axis=1, tiled=True)  5.96 us
  transfers between devices with their start and end apart: 8, of which 7 were waited for; matrix products, arithmetic and copies ran while one was open for 1% of the time, Pallas kernels for 0%

profile of v1, /device:TPU:0, one launch (start us, length us, event | category | flops | bytes accessed | tf_op | source)
XLA Modules:
  0.0 276.6 jit_solution(6097891200715248763)
XLA Ops:
  6.5 1.5 convert_element_type.65
  8.1 1.5 multiply_reduce_fusion
  9.6 0.8 dynamic_slice.21
  10.5 2.4 collective-permute-start
  13.9 2.0 fusion.8
  15.9 4.5 %all-to-all-start = ((bf16[4,64,512]{2,1,0:T(8,128)(2,1)}), bf16[4,64,512]{2,1,0:T(8,128)(2,1)S(1)}, u32[]{:S(2)}, u32[]{:S(2)}) async-start(bf16[4,64,512]{2,1,0:T(8,128)(2,1)} %bitcast), calls=%async_computation | async-start | bytes 524288 | tf_op jit(solution)/shard_map/all_to_all | solution.py:90
  20.5 6.0 %all-to-all-done = bf16[4,64,512]{2,1,0:T(8,128)(2,1)S(1)} async-done(((bf16[4,64,512]{2,1,0:T(8,128)(2,1)}), bf16[4,64,512]{2,1,0:T(8,128)(2,1)S(1)}, u32[]{:S(2)}, u32[]{:S(2)}) %all-to-all-start) | async-done | bytes 262176 | tf_op jit(solution)/shard_map/all_to_all | solution.py:90
  26.8 0.3 broadcast_in_dim.32
  27.4 0.5 convolution_convert_fusion.1
  27.9 33.1 %all_to_all.23 = bf16[8,32,2048]{2,1,0:T(8,128)(2,1)S(1)} all-to-all(bf16[8,32,2048]{2,1,0:T(8,128)(2,1)S(1)} %bitcast.35), channel_id=1, replica_groups=mesh['sp'=8,'tp'=4] {'sp'}, dimensions={0} | all-to-all | bytes 2097152 | tf_op jit(solution)/shard_map/all_to_all | solution.py:103
  61.0 1.3 collective-permute-start.1
  62.2 24.2 %collective-permute-done.1 = bf16[8,32,2048]{2,1,0:T(8,128)(2,1)S(1)} collective-permute-done((bf16[8,32,2048]{2,1,0:T(8,128)(2,1)S(1)}, bf16[8,32,2048]{2,1,0:T(8,128)(2,1)S(1)}, u32[]{:S(2)}, u32[]{:S(2)}) %collective-permute-start.1) | collective-permute-done | bytes 1048608 | tf_op jit(solution)/shard_map/ppermute | solution.py:17
  86.4 0.4 collective-permute-start.2
  86.8 24.3 %collective-permute-done.2 = bf16[8,32,2048]{2,1,0:T(8,128)(2,1)} collective-permute-done((bf16[8,32,2048]{2,1,0:T(8,128)(2,1)S(1)}, bf16[8,32,2048]{2,1,0:T(8,128)(2,1)}, u32[]{:S(2)}, u32[]{:S(2)}) %collective-permute-start.2) | collective-permute-done | bytes 1048608 | tf_op jit(solution)/shard_map/ppermute | solution.py:17
  111.1 24.0 %collective-permute-done.3 = bf16[8,32,2048]{2,1,0:T(8,128)(2,1)} collective-permute-done((bf16[8,32,2048]{2,1,0:T(8,128)(2,1)}, bf16[8,32,2048]{2,1,0:T(8,128)(2,1)}, u32[]{:S(2)}, u32[]{:S(2)}) %collective-permute-start.3) | collective-permute-done | bytes 1048608 | tf_op jit(solution)/shard_map/ppermute | solution.py:17
  135.1 1.3 constant_dynamic-update-slice_fusion.7
  136.4 1.3 constant_dynamic-update-slice_fusion.6
  137.9 1.3 constant_dynamic-update-slice_fusion.3
  139.2 1.3 constant_dynamic-update-slice_fusion.2
  140.6 0.6 constant_dynamic-slice_fusion
  141.2 1.4 copy-done.3
  142.7 4.5 %fusion.3 = f32[1024,896]{1,0:T(8,128)S(1)} fusion(bf16[1024,2048]{1,0:T(8,128)(2,1)S(1)} %bitcast.32, bf16[1,2048,896]{2,1,0:T(8,128)(2,1)S(1)} %copy-done.3), kind=kOutput, calls=%fused_computation.4 | convolution fusion | flops 3758096384 | bytes 11534336 | tf_op jit(solution)/shard_map/dot_general | solution.py:106
  147.2 4.7 %multiply_convert_fusion = bf16[1024,896]{1,0:T(8,128)(2,1)S(1)} fusion(f32[1024,896]{1,0:T(8,128)S(1)} %fusion.3, bf16[1024,2048]{1,0:T(8,128)(2,1)S(1)} %bitcast.33, bf16[1,2048,896]{2,1,0:T(8,128)(2,1)S(1)} %copy-done.4), kind=kOutput, calls=%fused_computation.6 | convolution fusion | flops 3763601408 | bytes 13369344 | tf_op jit(solution)/shard_map/dot_general | solution.py:107
  151.9 6.1 %convolution_convert_fusion = bf16[1024,2048]{1,0:T(8,128)(2,1)} fusion(bf16[1024,896]{1,0:T(8,128)(2,1)S(1)} %multiply_convert_fusion, bf16[1,896,2048]{2,1,0:T(8,128)(2,1)S(1)} %copy-done.5), kind=kOutput, calls=%fused_computation | convolution fusion | flops 3760193536 | bytes 9699328 | tf_op jit(solution)/shard_map/dot_general | solution.py:111
  157.9 52.3 %reduce-scatter.2.cloned.1.call-done = bf16[256,2048]{1,0:T(8,128)(2,1)} async-done(((bf16[1024,2048]{1,0:T(8,128)(2,1)}), bf16[256,2048]{1,0:T(8,128)(2,1)}) %reduce-scatter.2.cloned.1.call-update) | async-done | bytes 1048592 | tf_op jit(solution)/shard_map/reduce_scatter | solution.py:112
  210.2 4.6 %all-to-all-start.2 = ((bf16[8,32,2048]{2,1,0:T(8,128)(2,1)}), bf16[8,32,2048]{2,1,0:T(8,128)(2,1)S(1)}, u32[]{:S(2)}, u32[]{:S(2)}) async-start(bf16[8,32,2048]{2,1,0:T(8,128)(2,1)} %bitcast.37), calls=%async_computation.3 | async-start | bytes 2097152 | tf_op jit(solution)/shard_map/all_to_all | solution.py:119
  215.0 0.8 fusion.39
  215.9 0.3 fusion.30
  216.2 25.2 %all-to-all-done.2 = bf16[8,32,2048]{2,1,0:T(8,128)(2,1)S(1)} async-done(((bf16[8,32,2048]{2,1,0:T(8,128)(2,1)}), bf16[8,32,2048]{2,1,0:T(8,128)(2,1)S(1)}, u32[]{:S(2)}, u32[]{:S(2)}) %all-to-all-start.2) | async-done | bytes 1048608 | tf_op jit(solution)/shard_map/all_to_all | solution.py:119
  241.4 1.4 fusion.5
  242.8 24.6 %all-gather.2.cloned.1.call-done = bf16[256,2048]{1,0:T(8,128)(2,1)} async-done(((bf16[64,2048]{1,0:T(8,128)(2,1)}), bf16[256,2048]{1,0:T(8,128)(2,1)}) %all-gather.2.cloned.1.call-update) | async-done | bytes 1048592 | tf_op jit(solution)/shard_map/all_gather | solution.py:130
  267.4 2.3 copy.31
  (44 shorter events, 2.2 us)
Async XLA Ops:
  6.5 7.3 %copy-start = (bf16[512,512]{1,0:T(8,128)(2,1)S(1)}, bf16[512,512]{1,0:T(8,128)(2,1)}, u32[]{:S(2)}) copy-start(bf16[512,512]{1,0:T(8,128)(2,1)} %param.12) | copy-start | bytes 1572868
  6.5 6.4 %copy-start.2 = (s32[256,2]{0,1:T(2,128)S(1)}, s32[256,2]{0,1:T(2,128)}, u32[]{:S(2)}) copy-start(s32[256,2]{0,1:T(2,128)} %param.15) | copy-start | bytes 6148
  6.5 7.3 %copy-start.6 = (f32[512]{0:T(512)S(1)}, f32[512]{0:T(512)}, u32[]{:S(2)}) copy-start(f32[512]{0:T(512)} %param.13) | copy-start | bytes 6148
  10.5 3.3 %collective-permute-start = (bf16[16,512]{1,0:T(8,128)(2,1)S(1)}, bf16[16,512]{1,0:T(8,128)(2,1)S(1)}, u32[]{:S(2)}, u32[]{:S(2)}) collective-permute-start(bf16[16,512]{1,0:T(8,128)(2,1)S(1)} %slice.69), channel_id=1, source_target_pairs={{0,4},{4,8},{8,12},{12,16},{16,20},{20,24},{24,28},{1,5},{5,9},{9,... | collective-permute-start | bytes 49160 | tf_op jit(solution)/shard_map/ppermute | solution.py:31
  13.9 12.8 %copy-start.1 = (f32[2048]{0:T(1024)S(1)}, f32[2048]{0:T(1024)}, u32[]{:S(2)}) copy-start(f32[2048]{0:T(1024)} %param.14) | copy-start | bytes 24580
  15.9 10.5 %all-to-all-start = ((bf16[4,64,512]{2,1,0:T(8,128)(2,1)}), bf16[4,64,512]{2,1,0:T(8,128)(2,1)S(1)}, u32[]{:S(2)}, u32[]{:S(2)}) async-start(bf16[4,64,512]{2,1,0:T(8,128)(2,1)} %bitcast), calls=%async_computation | async-start | bytes 524288 | tf_op jit(solution)/shard_map/all_to_all | solution.py:90
  20.4 189.8 %reduce-scatter.2.cloned.1.call-start = ((), (), s32[]{:S(2)}) async-start(), calls=%async_computation.4 | async-start | bytes 5242880 | tf_op jit(solution)/shard_map/reduce_scatter | solution.py:112
  61.0 25.4 %collective-permute-start.1 = (bf16[8,32,2048]{2,1,0:T(8,128)(2,1)S(1)}, bf16[8,32,2048]{2,1,0:T(8,128)(2,1)S(1)}, u32[]{:S(2)}, u32[]{:S(2)}) collective-permute-start(bf16[8,32,2048]{2,1,0:T(8,128)(2,1)S(1)} %all_to_all.23), channel_id=1, source_target_pairs={{0,1},{1,2},{2,3},{3,0},{4,5},{5,6},{6,7},{7,4},{8,9},{9,10},{10,1... | collective-permute-start | bytes 3145736 | tf_op jit(solution)/shard_map/ppermute | solution.py:17
  86.4 24.7 %collective-permute-start.2 = (bf16[8,32,2048]{2,1,0:T(8,128)(2,1)S(1)}, bf16[8,32,2048]{2,1,0:T(8,128)(2,1)}, u32[]{:S(2)}, u32[]{:S(2)}) collective-permute-start(bf16[8,32,2048]{2,1,0:T(8,128)(2,1)S(1)} %collective-permute-done.1), channel_id=1, source_target_pairs={{0,1},{1,2},{2,3},{3,0},{4,5},{5,6},{6,7},{7,4},{8,9},{9,10},{10,1... | collective-permute-start | bytes 3145736 | tf_op jit(solution)/shard_map/ppermute | solution.py:17
  111.1 24.0 %collective-permute-start.3 = (bf16[8,32,2048]{2,1,0:T(8,128)(2,1)}, bf16[8,32,2048]{2,1,0:T(8,128)(2,1)}, u32[]{:S(2)}, u32[]{:S(2)}) collective-permute-start(bf16[8,32,2048]{2,1,0:T(8,128)(2,1)} %collective-permute-done.2), channel_id=1, source_target_pairs={{0,1},{1,2},{2,3},{3,0},{4,5},{5,6},{6,7},{7,4},{8,9},{9,10},{10,1... | collective-permute-start | bytes 3145736 | tf_op jit(solution)/shard_map/ppermute | solution.py:17
  140.6 2.0 copy-start.3
  142.7 4.5 %copy-start.4 = (bf16[1,2048,896]{2,1,0:T(8,128)(2,1)S(1)}, bf16[1,2048,896]{2,1,0:T(8,128)(2,1)}, u32[]{:S(2)}) copy-start(bf16[1,2048,896]{2,1,0:T(8,128)(2,1)} %param.18) | copy-start | bytes 11010052
  147.2 4.7 %copy-start.5 = (bf16[1,896,2048]{2,1,0:T(8,128)(2,1)S(1)}, bf16[1,896,2048]{2,1,0:T(8,128)(2,1)}, u32[]{:S(2)}) copy-start(bf16[1,896,2048]{2,1,0:T(8,128)(2,1)} %param.19) | copy-start | bytes 11010052
  210.2 31.2 %all-to-all-start.2 = ((bf16[8,32,2048]{2,1,0:T(8,128)(2,1)}), bf16[8,32,2048]{2,1,0:T(8,128)(2,1)S(1)}, u32[]{:S(2)}, u32[]{:S(2)}) async-start(bf16[8,32,2048]{2,1,0:T(8,128)(2,1)} %bitcast.37), calls=%async_computation.3 | async-start | bytes 2097152 | tf_op jit(solution)/shard_map/all_to_all | solution.py:119
  214.9 52.6 %all-gather.2.cloned.1.call-start = ((), (), s32[]{:S(2)}) async-start(), calls=%async_computation.5 | async-start | bytes 1310720 | tf_op jit(solution)/shard_map/all_gather | solution.py:130
Sparse Core Ops, SparseCore 0:
  158.1 52.1 reduce-scatter.1
  242.9 24.4 all-gather.1
